TPU v7x, 32 devices: a whole 2x2x4 slice. The times are simulated.
32 devices in a mesh: ep: 16 (over z, y, core), tp: 2 (over x).
Axes of the slice: x: 2, y: 2, z: 4, core: 2. Of those that a mesh axis runs over, the one named last changes fastest.
Arguments:
- tokens: bfloat16 [256, 2048], P('ep'), may hold values from -6 to 6
- lengths: int32 [256], P('ep'), may hold values from 256 to 1023
- cache: bfloat16 [256, 1024, 512], P('ep', None, 'tp'), may hold values from -6 to 6
- attn_gain: float32 [2048], replicated, may hold values from 0.1 to 1.9
- query_weight: bfloat16 [2048, 1024], P(None, 'tp'), may hold values from -0.125 to 0.125
- key_weight: bfloat16 [2048, 256], P(None, 'tp'), may hold values from -0.125 to 0.125
- value_weight: bfloat16 [2048, 256], P(None, 'tp'), may hold values from -0.125 to 0.125
- stick_bias: float32 [16], P('tp'), may hold values from -7 to -1
- out_weight: bfloat16 [1024, 2048], P('tp'), may hold values from -0.1875 to 0.1875
- ffn_gain: float32 [2048], replicated, may hold values from 0.1 to 1.9
- routes: int32 [256, 6], P('ep'), may hold values from 0 to 15, all different within a row; in each aligned block of 16 rows (0 to 15, 16 to 31, ...) at most 12 rows name the same one
- route_weights: float32 [256, 6], P('ep'), may hold values from 0.1 to 0.6
- expert_gate: bfloat16 [16, 2048, 1024], P('ep', None, 'tp'), may hold values from -0.125 to 0.125
- expert_up: bfloat16 [16, 2048, 1024], P('ep', None, 'tp'), may hold values from -0.125 to 0.125
- expert_down: bfloat16 [16, 1024, 2048], P('ep', 'tp'), may hold values from -0.1875 to 0.1875
- shared_gate: bfloat16 [2048, 512], P('ep', 'tp'), may hold values from -0.125 to 0.125
- shared_up: bfloat16 [2048, 512], P('ep', 'tp'), may hold values from -0.125 to 0.125
- shared_down: bfloat16 [512, 2048], P('tp'), may hold values from -0.25 to 0.25
- gate_vector: bfloat16 [2048], replicated, may hold values from -0.125 to 0.125
Outputs:
- layer_out: bfloat16 [256, 2048], P('ep', 'tp')
- new_kv: bfloat16 [256, 512], P('ep', 'tp')
Inputs may be any that keep to these rules, and one draw needn't show every extreme that they name: Each sequence's new token comes after its lengths cached positions. `routes`: each row names 6 different experts; among the 16 rows of one index of ep no expert is named by more than 12 rows.
All inputs are finite; a program needn't handle non-finite values.
Results may differ from a plain program's by a relative error of at most 0.012.
Values may be sent and summed in bfloat16 or wider, within the bound.
A program may use at most 64 MiB of HBM per device.

v0:
```python
import functools

import jax
import jax.numpy as jnp
from jax import lax
from jax.experimental import pallas as pl
from jax.experimental.pallas import tpu as pltpu
from jax.sharding import PartitionSpec as P

HEAD_DIM = 64
LANES = 128
epsilon = 1e-06
MESH = pl.DeviceIdType.MESH
F32 = jnp.float32
BF16 = jnp.bfloat16


def rms_scale(rows_in, gain_row):
    values_f = rows_in.astype(F32)
    return (
        values_f
        * lax.rsqrt(jnp.mean(values_f * values_f, axis=-1, keepdims=True) + epsilon)
        * gain_row
    )


def attend_kernel(groups, query_ref, span_ref, bias_ref, cache_ref, out_ref, held, logits, spread, sems):
    seqs, heads, _ = spread.shape
    tiles = spread.shape[2] // LANES
    group = heads // tiles
    first_half = lax.broadcasted_iota(jnp.int32, (seqs, LANES), 1) < HEAD_DIM
    length = cache_ref.shape[1]
    width = 256
    count = length // width
    copies = []
    for s in range(seqs):
        copy = pltpu.make_async_copy(cache_ref.at[s], held.at[s], sems.at[s])
        copy.start()
        copies.append(copy)
    spread[...] = jnp.zeros_like(spread)
    for h in range(heads):
        pair = query_ref[:, h // 2 * LANES : (h // 2 + 1) * LANES].astype(F32)
        if h % 2:
            pair = pltpu.roll(pair, HEAD_DIM, 1)
        tile = h // group * LANES
        spread[:, h, tile : tile + LANES] = jnp.where(first_half, pair, 0.0)
    table = (
        lax.broadcasted_iota(jnp.int32, (width, width), 0)
        >= lax.broadcasted_iota(jnp.int32, (width, width), 1)
    ).astype(F32)
    per_group = seqs // groups
    rows = per_group * heads
    for g in range(groups):
        first = g * per_group
        for s in range(first, first + per_group):
            copies[s].wait()
            logits[s * heads : (s + 1) * heads, :] = lax.dot_general(
                spread[s].astype(BF16), held[s], (((1,), (1,)), ((), ())), preferred_element_type=F32
            )
        span = slice(first * heads, first * heads + rows)
        row = lax.broadcasted_iota(jnp.int32, (rows, 1), 0)
        limit = jnp.zeros((rows, 1), jnp.int32)
        for s in range(per_group):
            limit = jnp.where(row // heads == s, span_ref[first + s], limit)
        offset = jnp.zeros((rows, 1), F32)
        for h in range(heads):
            offset = jnp.where(row % heads == h, bias_ref[h], offset)
        carried = jnp.zeros((rows, 1), F32)
        for b in range(count - 1, -1, -1):
            cols = slice(b * width, (b + 1) * width)
            z = logits[span, cols] * HEAD_DIM ** (-0.5) + offset
            position = lax.broadcasted_iota(jnp.int32, (rows, width), 1) + b * width
            usable = position < limit
            soft = jnp.where(usable, jnp.maximum(z, 0.0) + jnp.log1p(jnp.exp(-jnp.abs(z))), 0.0)
            behind = jnp.dot(soft, table, precision=lax.Precision.HIGHEST, preferred_element_type=F32)
            weight = jnp.where(usable, jnp.exp(z - behind - carried), 0.0)
            carried = carried + jnp.sum(soft, axis=1, keepdims=True)
            logits[span, cols] = weight
        for s in range(first, first + per_group):
            spread[s] = jnp.dot(
                logits[s * heads : (s + 1) * heads, :].astype(BF16),
                held[s],
                preferred_element_type=F32,
            )
    for i in range(heads // 2):
        pair = []
        for h in (2 * i, 2 * i + 1):
            tile = h // group * LANES
            pair.append(spread[:, h, tile : tile + LANES])
        both = jnp.where(first_half, pltpu.roll(pair[0], HEAD_DIM, 1), pair[1])
        out_ref[:, i * LANES : (i + 1) * LANES] = both.astype(BF16)


def attend(queries, lengths, bias, cache):
    seqs = queries.shape[0]
    heads = queries.shape[1] // HEAD_DIM
    length, lanes = cache.shape[1:]
    smem = pl.BlockSpec(memory_space=pltpu.SMEM)
    vmem = pl.BlockSpec(memory_space=pltpu.VMEM)
    return pl.pallas_call(
        functools.partial(attend_kernel, 2),
        out_shape=jax.ShapeDtypeStruct(queries.shape, BF16),
        in_specs=[vmem, smem, smem, pl.BlockSpec(memory_space=pl.ANY)],
        out_specs=vmem,
        scratch_shapes=[
            pltpu.VMEM((seqs, length, lanes), BF16),
            pltpu.VMEM((seqs * heads, length), F32),
            pltpu.VMEM((seqs, heads, lanes), F32),
            pltpu.SemaphoreType.DMA((seqs,)),
        ],
        compiler_params=pltpu.CompilerParams(vmem_limit_bytes=60 * 2**20),
    )(queries, lengths, bias, cache)


def reduce_rounds(own, landing, flip, zmasks, ymasks, cols, send_sem, recv_sem, sent):
    def push(block, goal, slot):
        copy = pltpu.make_async_remote_copy(
            src_ref=own.at[block, :, cols],
            dst_ref=landing.at[slot, :, cols],
            send_sem=send_sem.at[len(sent)],
            recv_sem=recv_sem.at[slot],
            device_id={"ep": flip(goal)},
            device_id_type=MESH,
        )
        copy.start()
        sent.append(copy)
        arrivals[slot] = copy

    def fold(block, slots):
        total = own[block, :, cols].astype(F32)
        for slot in slots:
            arrivals[slot].wait_recv()
            total = total + landing[slot, :, cols].astype(F32)
        return total

    arrivals = {}
    for y in (*ymasks, 0):
        for z in (*zmasks, 0):
            push(z + y + 1, 1, z + y)
    yield None
    for z in (*zmasks, 0):
        for y in ymasks:
            own[z + y, :, cols] = fold(z + y, [z + y]).astype(BF16)
            push(z + y, y, z + y + 1)
    yield None
    for z in zmasks:
        own[z, :, cols] = fold(z, [z, *(z + y + 1 for y in ymasks)]).astype(BF16)
        push(z, z, z + 1)
    yield None
    yield fold(0, [0, *(y + 1 for y in ymasks), *(z + 1 for z in zmasks)])


def mix_kernel(
    ranks_ep,
    ranks_tp,
    partial_ref,
    tokens_ref,
    gain_ref,
    vector_ref,
    routes_ref,
    portions_ref,
    sgate_ref,
    sup_ref,
    sdown_hbm,
    gate_hbm,
    up_hbm,
    down_hbm,
    out_ref,
    attn_in,
    residual_ref,
    gathered,
    hidden_ref,
    terms,
    terms_in,
    shared,
    shared_in,
    last,
    last_in,
    gate_w,
    up_w,
    down_w,
    sdown_w,
    load_sem,
    tp_send,
    tp_recv,
    ag_send,
    ag_recv,
    rs_send,
    rs_recv,
    sh_send,
    sh_recv,
    out_send,
    out_recv,
):
    me = lax.axis_index("ep")
    my_tp = lax.axis_index("tp")
    row_count, width = tokens_ref.shape
    experts = gate_w.shape[0]
    table_width = gathered.shape[2] - width
    all_rows = ranks_ep * row_count
    chips = ranks_ep // 2
    across = 1 << (chips.bit_length() - 1) // 2
    zmasks = [m * 2 * across for m in range(chips // across - 1, 0, -1)]
    ymasks = [m * 2 for m in range(across - 1, 0, -1)]

    def flip(mask):
        index = me
        weight = 1
        while weight <= mask:
            if mask & weight:
                index = index + (1 - 2 * ((me // weight) % 2)) * weight
            weight = weight * 2
        return index

    loads = []
    for i, (source, target) in enumerate(
        ((gate_hbm, gate_w), (up_hbm, up_w), (down_hbm, down_w), (sdown_hbm, sdown_w))
    ):
        load = pltpu.make_async_copy(source, target, load_sem.at[i])
        load.start()
        loads.append(load)

    barrier = pltpu.get_barrier_semaphore()
    for mask in (*zmasks, *ymasks, 1):
        pl.semaphore_signal(barrier, inc=1, device_id={"ep": flip(mask)}, device_id_type=MESH)
    for step in range(1, ranks_tp):
        pl.semaphore_signal(
            barrier, inc=1, device_id={"tp": lax.rem(my_tp + step, ranks_tp)}, device_id_type=MESH
        )
    pl.semaphore_wait(barrier, len(zmasks) + len(ymasks) + ranks_tp)

    swaps = []
    for step in range(1, ranks_tp):
        swap = pltpu.make_async_remote_copy(
            src_ref=partial_ref,
            dst_ref=attn_in.at[step - 1],
            send_sem=tp_send.at[step - 1],
            recv_sem=tp_recv.at[step - 1],
            device_id={"tp": lax.rem(my_tp + step, ranks_tp)},
            device_id_type=MESH,
        )
        swap.start()
        swaps.append(swap)

    lane = lax.broadcasted_iota(jnp.int32, (row_count, table_width), 1)
    stride = table_width // 2
    table = jnp.zeros((row_count, table_width), F32)
    route_ids = jnp.transpose(routes_ref[...])
    portions = jnp.transpose(portions_ref[...])
    for k in range(routes_ref.shape[0]):
        named = route_ids[:, k : k + 1]
        portion = portions[:, k : k + 1]
        high = portion.astype(BF16).astype(F32)
        table = jnp.where(lane == named, high, table)
        table = jnp.where(lane == named + stride, portion - high, table)
    gathered[0, :, width:] = table.astype(BF16)

    residual = partial_ref[...].astype(F32)
    for step in range(1, ranks_tp):
        swaps[step - 1].wait()
        residual = residual + attn_in[step - 1].astype(F32)
    residual = residual + tokens_ref[...].astype(F32)
    residual_ref[...] = residual
    normed = (
        residual
        * lax.rsqrt(jnp.mean(residual * residual, axis=-1, keepdims=True) + epsilon)
        * gain_ref[...]
    ).astype(BF16)
    gathered[0, :, :width] = normed

    sent = []
    arrivals = {}

    def share(block, goal):
        slot = block ^ goal
        copy = pltpu.make_async_remote_copy(
            src_ref=gathered.at[block],
            dst_ref=gathered.at[slot],
            send_sem=ag_send.at[len(sent)],
            recv_sem=ag_recv.at[slot],
            device_id={"ep": flip(goal)},
            device_id_type=MESH,
        )
        copy.start()
        sent.append(copy)
        arrivals[slot] = copy

    for mask in (*zmasks, *ymasks, 1):
        share(0, mask)
    mix_gate = jax.nn.sigmoid(
        jnp.sum(normed.astype(F32) * vector_ref[...].astype(F32).reshape(1, width), axis=1, keepdims=True)
    )
    for y in ymasks:
        arrivals[y].wait_recv()
        share(y, 1)
    for z in zmasks:
        arrivals[z].wait_recv()
        for y in ymasks:
            share(z, y)
        share(z, 1)
    for z in zmasks:
        for y in ymasks:
            arrivals[z + y].wait_recv()
            share(z + y, 1)
    for z in (*zmasks, 0):
        for y in (*ymasks, 0):
            arrivals[z + y + 1].wait_recv()

    shared_cols = sgate_ref.shape[1]
    depth = sgate_ref.shape[0]
    feature_at = pl.ds(pl.multiple_of(me * (width // ranks_ep) // depth * depth, depth), depth)
    features = gathered[:, :, feature_at].reshape(all_rows, depth)
    for i, part in enumerate((sgate_ref, sup_ref)):
        shared[:, :, i * shared_cols : (i + 1) * shared_cols] = (
            jnp.dot(features, part[...], preferred_element_type=F32)
            .astype(BF16)
            .reshape(ranks_ep, row_count, shared_cols)
        )
    shared_sent = []
    shared_rounds = reduce_rounds(
        shared,
        shared_in,
        flip,
        zmasks,
        ymasks,
        slice(None),
        sh_send,
        sh_recv,
        shared_sent,
    )
    next(shared_rounds)
    rows = gathered[:, :, :width].reshape(all_rows, width)
    route_cols = gathered[:, :, width:].reshape(all_rows, table_width).astype(F32)
    lanes = lax.broadcasted_iota(jnp.int32, route_cols.shape, 1)
    loads[0].wait()
    loads[1].wait()
    scales = []
    for j in range(experts):
        wanted = me * experts + j
        chosen = jnp.where((lanes == wanted) | (lanes == wanted + stride), route_cols, 0.0)
        scales.append(jnp.sum(chosen, axis=1, keepdims=True))
        gate_val = jnp.dot(rows, gate_w[j], preferred_element_type=F32)
        up_val = jnp.dot(rows, up_w[j], preferred_element_type=F32)
        hidden_ref[j] = (gate_val * jax.nn.sigmoid(gate_val) * up_val).astype(BF16)
    next(shared_rounds)
    loads[2].wait()
    loads[3].wait()
    half = width // 2
    term_sent = []
    rounds = []
    for s in range(2):
        cols = slice(s * half, (s + 1) * half)
        term = jnp.zeros((all_rows, half), F32)
        for j in range(experts):
            term = term + scales[j] * jnp.dot(
                hidden_ref[j], down_w[j, :, cols], preferred_element_type=F32
            )
        terms[:, :, cols] = term.astype(BF16).reshape(ranks_ep, row_count, half)
        term_sent.append([])
        rounds.append(
            reduce_rounds(
                terms,
                terms_in,
                flip,
                zmasks,
                ymasks,
                cols,
                rs_send.at[s],
                rs_recv.at[s],
                term_sent[s],
            )
        )
        next(rounds[s])
        if s == 0:
            next(shared_rounds)
    for turn in range(2):
        for s in range(2):
            next(rounds[s])
    total = next(shared_rounds)
    gate_sum = total[:, :shared_cols]
    up_sum = total[:, shared_cols:]
    shared_hidden = (gate_sum * jax.nn.sigmoid(gate_sum) * up_sum).astype(BF16)
    shared_term = mix_gate * jnp.dot(shared_hidden, sdown_w[...], preferred_element_type=F32)
    for s in range(2):
        cols = slice(s * half, (s + 1) * half)
        last[:, cols] = (next(rounds[s]) + shared_term[:, cols]).astype(BF16)
    quarter = width // ranks_tp

    def quarter_of(index):
        return pl.ds(pl.multiple_of(index * quarter, quarter), quarter)

    ends = []
    for step in range(1, ranks_tp):
        goal = lax.rem(my_tp + step, ranks_tp)
        end = pltpu.make_async_remote_copy(
            src_ref=last.at[:, quarter_of(goal)],
            dst_ref=last_in.at[step - 1],
            send_sem=out_send.at[step - 1],
            recv_sem=out_recv.at[step - 1],
            device_id={"tp": goal},
            device_id_type=MESH,
        )
        end.start()
        ends.append(end)
    for copy in (*sent, *shared_sent, *term_sent[0], *term_sent[1]):
        copy.wait_send()
    result = residual_ref[:, quarter_of(my_tp)] + last[:, quarter_of(my_tp)].astype(F32)
    for step in range(1, ranks_tp):
        ends[step - 1].wait()
        result = result + last_in[step - 1].astype(F32)
    out_ref[...] = result


def mix(
    ranks_ep,
    ranks_tp,
    attn_term,
    tokens,
    ffn_gain,
    gate_vector,
    routes,
    route_weights,
    shared_gate,
    shared_up,
    shared_down,
    expert_gate,
    expert_up,
    expert_down,
):
    row_count, width = tokens.shape
    grid = (ranks_ep, row_count)
    experts, _, hidden = expert_gate.shape
    shared_cols = shared_gate.shape[1]
    quarter = width // ranks_tp
    table_width = -(-2 * ranks_ep * experts // LANES) * LANES
    swaps = max(ranks_tp - 1, 1)
    vmem = pl.BlockSpec(memory_space=pltpu.VMEM)
    anywhere = pl.BlockSpec(memory_space=pl.ANY)
    dma = pltpu.SemaphoreType.DMA
    return pl.pallas_call(
        functools.partial(mix_kernel, ranks_ep, ranks_tp),
        out_shape=jax.ShapeDtypeStruct((row_count, quarter), F32),
        in_specs=[vmem] * 8 + [anywhere] * 4,
        out_specs=vmem,
        scratch_shapes=[
            pltpu.VMEM((swaps, row_count, width), BF16),
            pltpu.VMEM((row_count, width), F32),
            pltpu.VMEM((*grid, width + table_width), BF16),
            pltpu.VMEM((experts, ranks_ep * row_count, hidden), BF16),
            pltpu.VMEM((*grid, width), BF16),
            pltpu.VMEM((*grid, width), BF16),
            pltpu.VMEM((*grid, 2 * shared_cols), BF16),
            pltpu.VMEM((*grid, 2 * shared_cols), BF16),
            pltpu.VMEM((row_count, width), BF16),
            pltpu.VMEM((swaps, row_count, quarter), BF16),
            pltpu.VMEM(expert_gate.shape, BF16),
            pltpu.VMEM(expert_up.shape, BF16),
            pltpu.VMEM(expert_down.shape, BF16),
            pltpu.VMEM(shared_down.shape, BF16),
            dma((4,)),
            dma((swaps,)),
            dma((swaps,)),
            dma((ranks_ep,)),
            dma((ranks_ep,)),
            dma((2, ranks_ep)),
            dma((2, ranks_ep)),
            dma((ranks_ep,)),
            dma((ranks_ep,)),
            dma((swaps,)),
            dma((swaps,)),
        ],
        compiler_params=pltpu.CompilerParams(
            collective_id=0, has_side_effects=True, vmem_limit_bytes=60 * 2**20
        ),
    )(
        attn_term,
        tokens,
        ffn_gain.reshape(1, width),
        gate_vector,
        routes.T,
        route_weights.T,
        shared_gate,
        shared_up,
        shared_down,
        expert_gate,
        expert_up,
        expert_down,
    )


def shards(
    ranks_ep,
    ranks_tp,
    tokens,
    lengths,
    cache,
    attn_gain,
    query_weight,
    key_weight,
    value_weight,
    stick_bias,
    out_weight,
    ffn_gain,
    routes,
    route_weights,
    expert_gate,
    expert_up,
    expert_down,
    shared_gate,
    shared_up,
    shared_down,
    gate_vector,
):
    row_count = tokens.shape[0]
    normed = rms_scale(tokens, attn_gain).astype(BF16)
    queries = jnp.dot(normed, query_weight, preferred_element_type=F32).astype(BF16)
    key_rows = jnp.dot(normed, key_weight, preferred_element_type=F32).astype(BF16)
    value_rows = jnp.dot(normed, value_weight, preferred_element_type=F32).astype(BF16)
    heads = key_weight.shape[1] // HEAD_DIM
    new_kv = jnp.stack(
        [
            key_rows.reshape(row_count, heads, HEAD_DIM),
            value_rows.reshape(row_count, heads, HEAD_DIM),
        ],
        axis=2,
    ).reshape(row_count, heads * 2 * HEAD_DIM)
    heads_out = attend(queries, lengths, stick_bias, cache)
    attn_term = jnp.dot(
        heads_out, out_weight, preferred_element_type=F32
    ).astype(BF16)
    depth = shared_gate.shape[0]
    if depth % LANES:
        slot = lax.axis_index("ep") * depth % LANES
        wide = jnp.zeros((LANES, shared_gate.shape[1]), BF16)
        shared_gate = lax.dynamic_update_slice_in_dim(wide, shared_gate, slot, 0)
        shared_up = lax.dynamic_update_slice_in_dim(wide, shared_up, slot, 0)
    layer_out = mix(
        ranks_ep,
        ranks_tp,
        attn_term,
        tokens,
        ffn_gain,
        gate_vector,
        routes,
        route_weights,
        shared_gate,
        shared_up,
        shared_down,
        expert_gate,
        expert_up,
        expert_down,
    )
    return (layer_out.astype(BF16), new_kv)


def solution(mesh):
    placed = (
        P("ep", None),
        P("ep"),
        P("ep", None, "tp"),
        P(),
        P(None, "tp"),
        P(None, "tp"),
        P(None, "tp"),
        P("tp"),
        P("tp", None),
        P(),
        P("ep", None),
        P("ep", None),
        P("ep", None, "tp"),
        P("ep", None, "tp"),
        P("ep", "tp", None),
        P("ep", "tp"),
        P("ep", "tp"),
        P("tp", None),
        P(),
    )
    return jax.shard_map(
        functools.partial(shards, mesh.shape["ep"], mesh.shape["tp"]),
        mesh=mesh,
        in_specs=placed,
        out_specs=(P("ep", "tp"), P("ep", "tp")),
        check_vma=False,
    )
```

profile of v0, /device:TPU:0, one launch (start us, length us, event | category | flops | bytes accessed | tf_op | source)
XLA Modules:
  0.0 60.1 jit_solution(2759165085763370257)
XLA Ops:
  0.6 0.0 copy-start
  0.6 1.1 %fusion = f32[16]{0:T(128)S(1)} fusion(bf16[16,2048]{1,0:T(8,128)(2,1)} %tokens_ref.1), kind=kLoop, calls=%fused_computation.6 | loop fusion | flops 98288 | bytes 65600 | tf_op jit(solution)/shard_map/reduce_sum | solution.py:22
  1.8 2.7 %convolution_convert_fusion.1.query_ref = bf16[16,512]{1,0:T(8,128)(2,1)} fusion(bf16[2048,512]{1,0:T(8,128)(2,1)} %param.23, bf16[16,2048]{1,0:T(8,128)(2,1)} %tokens_ref.1, f32[2048]{0:T(1024)} %param.22, f32[16]{0:T(128)S(1)} %add_rsqrt_fusion), kind=kOutput, calls=%fused_computation.1 | convolution fusion | flops 33693696 | bytes 2187328 | tf_op jit(solution)/shard_map/dot_general | solution.py:516
  4.5 9.3 %shard_map.194 = bf16[16,512]{1,0:T(8,128)(2,1)} custom-call(bf16[16,512]{1,0:T(8,128)(2,1)} %convolution_convert_fusion.1.query_ref, s32[16]{0:T(128)} %span_ref.1, f32[8]{0:T(128)} %bias_ref.1, bf16[16,1024,256]{2,1,0:T(8,128)(2,1)} %cache_ref.1), custom_call_target="tpu_custom_call" | custom-call | tf_op jit(solution)/shard_map/pallas_call | solution.py:100
  13.7 0.0 copy-done
  13.7 1.7 %convolution_convert_fusion.partial_ref = bf16[16,2048]{1,0:T(8,128)(2,1)} fusion(bf16[16,512]{1,0:T(8,128)(2,1)} %shard_map.194, bf16[512,2048]{1,0:T(8,128)(2,1)S(1)} %copy-done), kind=kOutput, calls=%fused_computation | convolution fusion | flops 33587200 | bytes 2179072 | tf_op jit(solution)/shard_map/dot_general | solution.py:528
  15.5 0.0 copy-start.1
  15.5 0.0 copy-start.2
  15.5 0.0 copy-start.4
  15.5 0.0 copy-start.3
  15.5 41.7 %shard_map.195 = f32[16,1024]{1,0:T(8,128)} custom-call(bf16[16,2048]{1,0:T(8,128)(2,1)} %convolution_convert_fusion.partial_ref, bf16[16,2048]{1,0:T(8,128)(2,1)} %tokens_ref.1, f32[1,2048]{1,0:T(1,128)} %bitcast.8, bf16[2048]{0:T(1024)(128)(2,1)} %vector_ref.1, s32[6,16]{1,0:T(8,128)} %bitcast.9, f32[6,16]{1,0:T(8,128)} %bitcast.10, ...), custom_call_target="tpu_custom_call" | custom-call | tf_op jit(solution)/shard_map/pallas_call | solution.py:440
  57.2 1.5 %convert_element_type.25 = bf16[16,1024]{1,0:T(8,128)(2,1)} convert(f32[16,1024]{1,0:T(8,128)} %shard_map.195) | non-fusion elementwise | flops 16384 | bytes 98304 | tf_op jit(solution)/shard_map/convert_element_type | solution.py:553
  58.7 0.0 copy-done.1
  58.7 0.0 copy-done.2
  58.7 0.0 copy-done.4
  58.7 0.2 convolution_convert_fusion.2
  58.9 0.1 stack_reshape.7
  59.0 0.0 copy-done.3
  59.0 0.2 convolution_convert_fusion.3
  59.3 0.1 stack_reshape.6
  59.4 0.7 %reshape.20 = bf16[16,256]{1,0:T(8,128)(2,1)} reshape(bf16[16,2,2,64]{3,2,1,0:T(2,128)(2,1)S(1)} %copy.21) | data formatting | bytes 16384 | tf_op jit(solution)/shard_map/reshape | solution.py:526
  (3 shorter events, 0.1 us)
Async XLA Ops:
  0.6 13.1 %copy-start = (bf16[512,2048]{1,0:T(8,128)(2,1)S(1)}, bf16[512,2048]{1,0:T(8,128)(2,1)}, u32[]{:S(2)}) copy-start(bf16[512,2048]{1,0:T(8,128)(2,1)} %param.27) | copy-start | bytes 6291460
  15.5 43.2 %copy-start.1 = (bf16[16,2048]{1,0:T(8,128)(2,1)S(1)}, bf16[16,2048]{1,0:T(8,128)(2,1)}, u32[]{:S(2)}) copy-start(bf16[16,2048]{1,0:T(8,128)(2,1)} %tokens_ref.1) | copy-start | bytes 196612
  15.5 43.2 %copy-start.2 = (bf16[2048,128]{1,0:T(8,128)(2,1)S(1)}, bf16[2048,128]{1,0:T(8,128)(2,1)}, u32[]{:S(2)}) copy-start(bf16[2048,128]{1,0:T(8,128)(2,1)} %param.25) | copy-start | bytes 1572868
  15.5 43.2 %copy-start.4 = (f32[2048]{0:T(1024)S(1)}, f32[2048]{0:T(1024)}, u32[]{:S(2)}) copy-start(f32[2048]{0:T(1024)} %param.22) | copy-start | bytes 24580
  15.5 43.5 %copy-start.3 = (bf16[2048,128]{1,0:T(8,128)(2,1)S(1)}, bf16[2048,128]{1,0:T(8,128)(2,1)}, u32[]{:S(2)}) copy-start(bf16[2048,128]{1,0:T(8,128)(2,1)} %param.24) | copy-start | bytes 1572868
where the time goes:
time: 60.4 us; the launch traced here: 60.1 us
  Pallas kernels  51 us (84%)
  matrix products  4.89 us (8%)
  other arithmetic  2.63 us (4%)
  local copies, waits for them, and re-layouts  0.89 us (1%)
  between operations  0.69 us (1%)
    pallas_call x1, Pallas kernels, mix(): pl.pallas_call(functools.partial(mix_kernel, ranks_ep, ranks_tp), out_sha...  41.7 us
    pallas_call x1, Pallas kernels, attend(): pl.pallas_call(functools.partial(attend_kernel, 2), out_shape=jax.ShapeDt...  9.26 us
    dot_general x1, matrix products, shards(): jnp.dot(normed, query_weight, preferred_element_type=F32).astype(BF16)  2.69 us
    dot_general x1, matrix products, shards(): jnp.dot(heads_out, out_weight, preferred_element_type=F32).astype(BF16)  1.72 us
    convert_element_type x1, other arithmetic, shards(): return (layer_out.astype(BF16), new_kv)  1.46 us

commit v1 on v0

v1 whole, which is shorter than its diff:
```python
import functools

import jax
import jax.numpy as jnp
from jax import lax
from jax.experimental import pallas as pl
from jax.experimental.pallas import tpu as pltpu
from jax.sharding import PartitionSpec as P

HEAD_DIM = 64
LANES = 128
GROUPS = 2
CHUNKS = 2
epsilon = 1e-06
MESH = pl.DeviceIdType.MESH
F32 = jnp.float32
BF16 = jnp.bfloat16


def normalise(values, gain):
    return (
        values * lax.rsqrt(jnp.mean(values * values, axis=-1, keepdims=True) + epsilon) * gain
    ).astype(BF16)


def layer_kernel(
    ranks_ep,
    ranks_tp,
    tokens_hbm,
    lengths_hbm,
    cache_hbm,
    attn_gain_hbm,
    query_hbm,
    key_hbm,
    value_hbm,
    bias_hbm,
    out_hbm,
    ffn_gain_hbm,
    routes_hbm,
    portions_hbm,
    gate_hbm,
    up_hbm,
    down_hbm,
    sgate_hbm,
    sup_hbm,
    sdown_hbm,
    vector_hbm,
    out_ref,
    kv_ref,
    tokens_ref,
    span_ref,
    held,
    attn_gain_ref,
    query_w,
    key_w,
    value_w,
    bias_ref,
    out_w,
    ffn_gain_ref,
    routes_ref,
    portions_ref,
    gate_w,
    up_w,
    down_w,
    sgate_w,
    sup_w,
    sdown_w,
    vector_ref,
    normed_ref,
    logits,
    spread,
    partial,
    attn_in,
    residual_ref,
    gathered,
    hidden_ref,
    terms,
    core_in,
    mid,
    x_in,
    fin,
    fin_in,
    sh_own,
    sh_in,
    sh_mid,
    sh_fin,
    sh_out,
    sh_x,
    load_sem,
    cache_sem,
    swap_send,
    swap_recv,
    ag_send,
    ag_recv,
    core_send,
    core_recv,
    x_send,
    x_recv,
    fin_send,
    fin_recv,
    shc_send,
    shc_recv,
    shf_send,
    shf_recv,
    shx_send,
    shx_recv,
):
    me = lax.axis_index("ep")
    my_tp = lax.axis_index("tp")
    row_count, width = tokens_ref.shape
    groups = gathered.shape[0]
    rows = row_count // groups
    experts = gate_w.shape[0]
    table_width = gathered.shape[2] - width
    all_rows = ranks_ep * rows
    half = ranks_ep // 2
    half_rows = half * rows
    heads = spread.shape[1]
    tiles = spread.shape[2] // LANES
    group = heads // tiles
    quarter = width // ranks_tp
    chunks = terms.shape[1]
    chunk_width = quarter // chunks
    chips = ranks_ep // 2
    across = 1 << (chips.bit_length() - 1) // 2
    zmasks = [m * 2 * across for m in range(chips // across - 1, 0, -1)]
    ymasks = [m * 2 for m in range(across - 1, 0, -1)]
    away = [z + y for z in (*zmasks, 0) for y in (*ymasks, 0) if z + y]

    def flip(mask):
        index = me
        weight = 1
        while weight <= mask:
            if mask & weight:
                index = index + (1 - 2 * ((me // weight) % 2)) * weight
            weight = weight * 2
        return index

    def peer(step):
        return lax.rem(my_tp + step, ranks_tp)

    loads = {}

    def load(name, source, target):
        copy = pltpu.make_async_copy(source, target, load_sem.at[len(loads)])
        copy.start()
        loads[name] = copy

    caches = []

    def load_caches(g):
        for s in range(g * rows, (g + 1) * rows):
            copy = pltpu.make_async_copy(cache_hbm.at[s], held.at[s], cache_sem.at[s])
            copy.start()
            caches.append(copy)

    load("tokens", tokens_hbm, tokens_ref)
    load("attn_gain", attn_gain_hbm, attn_gain_ref)
    load("query", query_hbm, query_w)
    load("lengths", lengths_hbm, span_ref)
    load("bias", bias_hbm, bias_ref)
    load_caches(0)
    barrier = pltpu.get_barrier_semaphore()
    for mask in (*away, 1):
        pl.semaphore_signal(barrier, inc=1, device_id={"ep": flip(mask)}, device_id_type=MESH)
    for step in range(1, ranks_tp):
        pl.semaphore_signal(barrier, inc=1, device_id={"tp": peer(step)}, device_id_type=MESH)

    loads["tokens"].wait()
    loads["attn_gain"].wait()
    normed_ref[...] = normalise(tokens_ref[...].astype(F32), attn_gain_ref[...])
    loads["query"].wait()
    load("out", out_hbm, out_w)
    for g in range(1, groups):
        load_caches(g)
    load("ffn_gain", ffn_gain_hbm, ffn_gain_ref)
    load("routes", routes_hbm, routes_ref)
    load("portions", portions_hbm, portions_ref)
    load("vector", vector_hbm, vector_ref)
    queries = jnp.dot(normed_ref[...], query_w[...], preferred_element_type=F32).astype(BF16).astype(F32)
    queries = queries * HEAD_DIM ** (-0.5)
    spread[...] = jnp.zeros_like(spread)
    first_half = lax.broadcasted_iota(jnp.int32, (row_count, LANES), 1) < HEAD_DIM
    for h in range(heads):
        pair = queries[:, h // 2 * LANES : (h // 2 + 1) * LANES]
        if h % 2:
            pair = pltpu.roll(pair, HEAD_DIM, 1)
        tile = h // group * LANES
        spread[:, h, tile : tile + LANES] = jnp.where(first_half, pair, 0.0)
    loads["lengths"].wait()
    loads["bias"].wait()

    length = held.shape[1]
    block = 256
    count = length // block
    lines = rows * heads

    def attend(g):
        first = g * rows
        for s in range(first, first + rows):
            caches[s].wait()
        for s in range(first, first + rows):
            logits[(s - first) * heads : (s - first + 1) * heads, :] = lax.dot_general(
                spread[s].astype(BF16), held[s], (((1,), (1,)), ((), ())), preferred_element_type=F32
            )
        row = lax.broadcasted_iota(jnp.int32, (lines, 1), 0)
        limit = jnp.zeros((lines, 1), jnp.int32)
        for s in range(rows):
            limit = jnp.where(row // heads == s, span_ref[first + s], limit)
        offset = jnp.zeros((lines, 1), F32)
        for h in range(heads):
            offset = jnp.where(row % heads == h, bias_ref[h], offset)
        table = (
            lax.broadcasted_iota(jnp.int32, (block, block), 0)
            >= lax.broadcasted_iota(jnp.int32, (block, block), 1)
        ).astype(F32).astype(BF16)
        position = lax.broadcasted_iota(jnp.int32, (lines, block), 1)
        parts = []
        for b in range(count):
            cols = slice(b * block, (b + 1) * block)
            z = logits[:, cols] + offset
            usable = position + b * block < limit
            soft = jnp.where(usable, jnp.maximum(z, 0.0) + jnp.log(1.0 + jnp.exp(-jnp.abs(z))), 0.0)
            logits[:, cols] = jnp.where(usable, z, -1e30)
            high = soft.astype(BF16)
            parts.append((high, (soft - high.astype(F32)).astype(BF16)))
        sums = [
            jnp.dot(high, table, preferred_element_type=F32)
            + jnp.dot(low, table, preferred_element_type=F32)
            for high, low in parts
        ]
        carried = jnp.zeros((lines, 1), F32)
        for b in range(count - 1, -1, -1):
            cols = slice(b * block, (b + 1) * block)
            logits[:, cols] = jnp.exp(logits[:, cols] - sums[b] - carried)
            carried = carried + sums[b][:, :1]
        for s in range(first, first + rows):
            spread[s] = jnp.dot(
                logits[(s - first) * heads : (s - first + 1) * heads, :].astype(BF16),
                held[s],
                preferred_element_type=F32,
            )
        upper = lax.broadcasted_iota(jnp.int32, (rows, LANES), 1) < HEAD_DIM
        gathered_heads = []
        for i in range(heads // 2):
            pair = []
            for h in (2 * i, 2 * i + 1):
                tile = h // group * LANES
                pair.append(spread[first : first + rows, h, tile : tile + LANES])
            gathered_heads.append(jnp.where(upper, pltpu.roll(pair[0], HEAD_DIM, 1), pair[1]))
        return jnp.concatenate(gathered_heads, axis=1).astype(BF16)

    swaps = {}

    def swap(g, heads_out):
        partial[g] = jnp.dot(heads_out, out_w[...], preferred_element_type=F32).astype(BF16)
        for step in range(1, ranks_tp):
            copy = pltpu.make_async_remote_copy(
                src_ref=partial.at[g],
                dst_ref=attn_in.at[g, step - 1],
                send_sem=swap_send.at[g, step - 1],
                recv_sem=swap_recv.at[g, step - 1],
                device_id={"tp": peer(step)},
                device_id_type=MESH,
            )
            copy.start()
            swaps[g, step] = copy

    def spot(mask):
        return (mask % 2 * half + mask // 2) * rows

    sent = []
    arrivals = {}
    shares = [0] * groups

    def share(g, source, goal):
        slot = source ^ goal
        copy = pltpu.make_async_remote_copy(
            src_ref=gathered.at[g, pl.ds(spot(source), rows)],
            dst_ref=gathered.at[g, pl.ds(spot(slot), rows)],
            send_sem=ag_send.at[g, shares[g]],
            recv_sem=ag_recv.at[g, slot],
            device_id={"ep": flip(goal)},
            device_id_type=MESH,
        )
        copy.start()
        shares[g] += 1
        sent.append(copy)
        arrivals[g, slot] = copy

    def spread_tokens(g):
        own = slice(g * rows, (g + 1) * rows)
        residual = partial[g].astype(F32)
        for step in range(1, ranks_tp):
            swaps[g, step].wait_recv()
            residual = residual + attn_in[g, step - 1].astype(F32)
        residual = residual + tokens_ref[own, :].astype(F32)
        residual_ref[own, :] = residual
        normed = normalise(residual, ffn_gain_ref[...])
        gathered[g, 0:rows, :width] = normed
        for mask in (*zmasks, *ymasks, 1):
            share(g, 0, mask)
        return jax.nn.sigmoid(
            jnp.sum(
                normed.astype(F32) * vector_ref[...].astype(F32).reshape(1, width), axis=1, keepdims=True
            )
        )

    def pass_near(g):
        for z in zmasks:
            arrivals[g, z].wait_recv()
            for y in ymasks:
                share(g, z, y)
            share(g, z, 1)
        for y in ymasks:
            arrivals[g, y].wait_recv()
            share(g, y, 1)

    def pass_far(g):
        for z in zmasks:
            for y in ymasks:
                arrivals[g, z + y].wait_recv()
                share(g, z + y, 1)

    def collect(g):
        for mask in (*away, 0):
            arrivals[g, mask + 1].wait_recv()

    shared_cols = sgate_w.shape[1]
    depth = sgate_w.shape[0]

    def push(source, target, send_sem, recv_sem, device):
        copy = pltpu.make_async_remote_copy(
            src_ref=source,
            dst_ref=target,
            send_sem=send_sem,
            recv_sem=recv_sem,
            device_id=device,
            device_id_type=MESH,
        )
        copy.start()
        sent.append(copy)
        return copy

    moves = {}

    def shared_in(g):
        feature_at = pl.ds(pl.multiple_of(me * (width // ranks_ep) // depth * depth, depth), depth)
        features = gathered[g, :, feature_at]
        for i, part in enumerate((sgate_w, sup_w)):
            sh_own[g, :, i * shared_cols : (i + 1) * shared_cols] = jnp.dot(
                features, part[...], preferred_element_type=F32
            ).astype(BF16)
        moves["shc", g] = push(
            sh_own.at[g, pl.ds(half_rows, half_rows)],
            sh_in.at[g],
            shc_send.at[g],
            shc_recv.at[g],
            {"ep": flip(1)},
        )

    def expert_in(g):
        inputs = gathered[g, :, :width]
        route_cols = gathered[g, :, width:].astype(F32)
        lanes = lax.broadcasted_iota(jnp.int32, route_cols.shape, 1)
        stride = table_width // 2
        scales = []
        for j in range(experts):
            wanted = me * experts + j
            chosen = jnp.where((lanes == wanted) | (lanes == wanted + stride), route_cols, 0.0)
            scales.append(jnp.sum(chosen, axis=1, keepdims=True))
            gate_val = jnp.dot(inputs, gate_w[j], preferred_element_type=F32)
            up_val = jnp.dot(inputs, up_w[j], preferred_element_type=F32)
            hidden_ref[g, j] = (gate_val * jax.nn.sigmoid(gate_val) * up_val).astype(BF16)
        return scales

    def expert_out(g, scales):
        for c in range(chunks):
            for step in range(ranks_tp):
                start = peer(step) * quarter + c * chunk_width
                cols = pl.ds(pl.multiple_of(start, chunk_width), chunk_width)
                term = jnp.zeros((all_rows, chunk_width), F32)
                for j in range(experts):
                    term = term + scales[j] * jnp.dot(
                        hidden_ref[g, j], down_w[j, :, cols], preferred_element_type=F32
                    )
                terms[g, c, step] = term.astype(BF16)
            moves["core", g, c] = push(
                terms.at[g, c, :, pl.ds(half_rows, half_rows)],
                core_in.at[g, c],
                core_send.at[g, c],
                core_recv.at[g, c],
                {"ep": flip(1)},
            )

    def shared_far(g):
        moves["shc", g].wait_recv()
        sh_mid[g] = (sh_own[g, :half_rows].astype(F32) + sh_in[g].astype(F32)).astype(BF16)
        for i, mask in enumerate(away):
            moves["shf", g, i] = push(
                sh_mid.at[g, pl.ds(spot(mask), rows)],
                sh_fin.at[g, i],
                shf_send.at[g, i],
                shf_recv.at[g, i],
                {"ep": flip(mask)},
            )

    def cross(g):
        for c in range(chunks):
            moves["core", g, c].wait_recv()
            for step in (*range(1, ranks_tp), 0):
                mid[g, c, step] = (
                    terms[g, c, step, :half_rows].astype(F32) + core_in[g, c, step].astype(F32)
                ).astype(BF16)
                if step:
                    moves["x", g, c, step] = push(
                        mid.at[g, c, step],
                        x_in.at[g, c, step - 1],
                        x_send.at[g, c, step - 1],
                        x_recv.at[g, c, step - 1],
                        {"tp": peer(step)},
                    )

    def deliver(g):
        for c in range(chunks):
            total = mid[g, c, 0].astype(F32)
            for step in range(1, ranks_tp):
                moves["x", g, c, step].wait_recv()
                total = total + x_in[g, c, step - 1].astype(F32)
            fin[g, c] = total.astype(BF16)
            for i, mask in enumerate(away):
                moves["fin", g, c, i] = push(
                    fin.at[g, c, pl.ds(spot(mask), rows)],
                    fin_in.at[g, c, i],
                    fin_send.at[g, c, i],
                    fin_recv.at[g, c, i],
                    {"ep": flip(mask)},
                )

    def quarter_of(index):
        return pl.ds(pl.multiple_of(index * quarter, quarter), quarter)

    def shared_end(g):
        total = sh_mid[g, 0:rows].astype(F32)
        for i in range(len(away)):
            moves["shf", g, i].wait_recv()
            total = total + sh_fin[g, i].astype(F32)
        gate_sum = total[:, :shared_cols]
        up_sum = total[:, shared_cols:]
        hidden = (gate_sum * jax.nn.sigmoid(gate_sum) * up_sum).astype(BF16)
        for step in range(1, ranks_tp):
            sh_out[g, step] = jnp.dot(
                hidden, sdown_w[:, quarter_of(peer(step))], preferred_element_type=F32
            ).astype(BF16)
            moves["shx", g, step] = push(
                sh_out.at[g, step],
                sh_x.at[g, step - 1],
                shx_send.at[g, step - 1],
                shx_recv.at[g, step - 1],
                {"tp": peer(step)},
            )
        sh_out[g, 0] = jnp.dot(
            hidden, sdown_w[:, quarter_of(my_tp)], preferred_element_type=F32
        ).astype(BF16)

    def finish(g, mix_gate):
        own = slice(g * rows, (g + 1) * rows)
        shared = sh_out[g, 0].astype(F32)
        for step in range(1, ranks_tp):
            moves["shx", g, step].wait_recv()
            shared = shared + sh_x[g, step - 1].astype(F32)
        base = residual_ref[own, quarter_of(my_tp)] + mix_gate * shared
        for c in range(chunks):
            cols = slice(c * chunk_width, (c + 1) * chunk_width)
            total = fin[g, c, 0:rows].astype(F32)
            for i in range(len(away)):
                moves["fin", g, c, i].wait_recv()
                total = total + fin_in[g, c, i].astype(F32)
            out_ref[own, cols] = (base[:, cols] + total).astype(out_ref.dtype)

    scope = jax.named_scope
    mix_gates = []
    scales = []
    for g in range(groups):
        with scope(f"attend{g}"):
            heads_out = attend(g)
        if g == 0:
            loads["out"].wait()
            load("key", key_hbm, key_w)
            load("value", value_hbm, value_w)
            load("sgate", sgate_hbm, sgate_w)
            load("sup", sup_hbm, sup_w)
            load("gate", gate_hbm, gate_w)
            load("up", up_hbm, up_w)
            load("down", down_hbm, down_w)
            load("sdown", sdown_hbm, sdown_w)
            with scope("barrier"):
                pl.semaphore_wait(barrier, len(away) + ranks_tp)
        with scope(f"swap{g}"):
            swap(g, heads_out)

    lane = lax.broadcasted_iota(jnp.int32, (row_count, table_width), 1)
    stride = table_width // 2
    table = jnp.zeros((row_count, table_width), F32)
    loads["routes"].wait()
    loads["portions"].wait()
    route_ids = jnp.transpose(routes_ref[...])
    portions = jnp.transpose(portions_ref[...])
    for k in range(routes_ref.shape[0]):
        named = route_ids[:, k : k + 1]
        portion = portions[:, k : k + 1]
        high = portion.astype(BF16).astype(F32)
        table = jnp.where(lane == named, high, table)
        table = jnp.where(lane == named + stride, portion - high, table)
    for g in range(groups):
        gathered[g, 0:rows, width:] = table[g * rows : (g + 1) * rows].astype(BF16)
    loads["ffn_gain"].wait()
    loads["vector"].wait()
    for g in range(groups):
        with scope(f"tokens{g}"):
            mix_gates.append(spread_tokens(g))
        if g == 0:
            with scope("kv"):
                loads["key"].wait()
                loads["value"].wait()
                key_rows = jnp.dot(normed_ref[...], key_w[...], preferred_element_type=F32)
                value_rows = jnp.dot(normed_ref[...], value_w[...], preferred_element_type=F32)
                pieces = []
                for h in range(key_w.shape[1] // HEAD_DIM):
                    cols = slice(h * HEAD_DIM, (h + 1) * HEAD_DIM)
                    pieces += [key_rows[:, cols], value_rows[:, cols]]
                kv_ref[...] = jnp.concatenate(pieces, axis=1).astype(BF16)
    for name in ("sgate", "sup", "gate", "up", "down", "sdown"):
        loads[name].wait()
    for g in range(groups):
        with scope(f"near{g}"):
            pass_near(g)
    for g in range(groups):
        if g == 0:
            with scope(f"far{g}"):
                pass_far(g)
        with scope(f"collect{g}"):
            collect(g)
        with scope(f"shin{g}"):
            shared_in(g)
        with scope(f"expin{g}"):
            scales.append(expert_in(g))
        if g + 1 < groups:
            with scope(f"far{g+1}"):
                pass_far(g + 1)
        with scope(f"expout{g}"):
            expert_out(g, scales[g])
        with scope(f"shfar{g}"):
            shared_far(g)
        if g + 1 < groups:
            with scope(f"cross{g}"):
                cross(g)
    for g in range(groups - 1):
        with scope(f"deliver{g}"):
            deliver(g)
    with scope(f"cross{groups-1}"):
        cross(groups - 1)
    for g in range(groups):
        with scope(f"shend{g}"):
            shared_end(g)
    with scope(f"deliver{groups-1}"):
        deliver(groups - 1)
    for g in range(groups):
        with scope(f"finish{g}"):
            finish(g, mix_gates[g])
    with scope("sends"):
        for copy in swaps.values():
            copy.wait_send()
        for copy in sent:
            copy.wait_send()


def layer(ranks_ep, ranks_tp, *operands):
    tokens, lengths, cache, _, query, key, value, bias, out_weight = operands[:9]
    _, routes, portions, gate, up, down, sgate, sup, sdown, vector = operands[9:]
    row_count, width = tokens.shape
    groups = GROUPS
    rows = row_count // groups
    experts, _, hidden = gate.shape
    shared_cols = sgate.shape[1]
    quarter = width // ranks_tp
    chunks = CHUNKS
    chunk_width = quarter // chunks
    heads = query.shape[1] // HEAD_DIM
    length, lanes = cache.shape[1:]
    table_width = -(-2 * ranks_ep * experts // LANES) * LANES
    swaps = max(ranks_tp - 1, 1)
    all_rows = ranks_ep * rows
    half_rows = all_rows // 2
    away = max(ranks_ep // 2 - 1, 1)
    vmem = pl.BlockSpec(memory_space=pltpu.VMEM)
    hbm = pl.BlockSpec(memory_space=pltpu.HBM)
    dma = pltpu.SemaphoreType.DMA

    def store(*shape, dtype=BF16):
        return pltpu.VMEM(shape, dtype)

    def like(array):
        return pltpu.VMEM(array.shape, array.dtype)

    return pl.pallas_call(
        functools.partial(layer_kernel, ranks_ep, ranks_tp),
        out_shape=(
            jax.ShapeDtypeStruct((row_count, quarter), BF16),
            jax.ShapeDtypeStruct((row_count, 2 * key.shape[1]), BF16),
        ),
        in_specs=[hbm] * len(operands),
        out_specs=(vmem, vmem),
        scratch_shapes=[
            like(tokens),
            pltpu.SMEM(lengths.shape, lengths.dtype),
            like(cache),
            like(operands[3]),
            like(query),
            like(key),
            like(value),
            pltpu.SMEM(bias.shape, bias.dtype),
            like(out_weight),
            like(operands[9]),
            like(routes),
            like(portions),
            like(gate),
            like(up),
            like(down),
            like(sgate),
            like(sup),
            like(sdown),
            like(vector),
            store(row_count, width),
            store(rows * heads, length, dtype=F32),
            store(row_count, heads, lanes, dtype=F32),
            store(groups, rows, width),
            store(groups, swaps, rows, width),
            store(row_count, width, dtype=F32),
            store(groups, all_rows, width + table_width),
            store(groups, experts, all_rows, hidden),
            store(groups, chunks, ranks_tp, all_rows, chunk_width),
            store(groups, chunks, ranks_tp, half_rows, chunk_width),
            store(groups, chunks, ranks_tp, half_rows, chunk_width),
            store(groups, chunks, swaps, half_rows, chunk_width),
            store(groups, chunks, half_rows, chunk_width),
            store(groups, chunks, away, rows, chunk_width),
            store(groups, all_rows, 2 * shared_cols),
            store(groups, half_rows, 2 * shared_cols),
            store(groups, half_rows, 2 * shared_cols),
            store(groups, away, rows, 2 * shared_cols),
            store(groups, ranks_tp, rows, quarter),
            store(groups, swaps, rows, quarter),
            dma((24,)),
            dma((row_count,)),
            dma((groups, swaps)),
            dma((groups, swaps)),
            dma((groups, ranks_ep)),
            dma((groups, ranks_ep)),
            dma((groups, chunks)),
            dma((groups, chunks)),
            dma((groups, chunks, swaps)),
            dma((groups, chunks, swaps)),
            dma((groups, chunks, away)),
            dma((groups, chunks, away)),
            dma((groups,)),
            dma((groups,)),
            dma((groups, away)),
            dma((groups, away)),
            dma((groups, swaps)),
            dma((groups, swaps)),
        ],
        compiler_params=pltpu.CompilerParams(
            collective_id=0, has_side_effects=True, vmem_limit_bytes=60 * 2**20
        ),
    )(*operands)


def shards(
    ranks_ep,
    ranks_tp,
    tokens,
    lengths,
    cache,
    attn_gain,
    query_weight,
    key_weight,
    value_weight,
    stick_bias,
    out_weight,
    ffn_gain,
    routes,
    route_weights,
    expert_gate,
    expert_up,
    expert_down,
    shared_gate,
    shared_up,
    shared_down,
    gate_vector,
):
    width = tokens.shape[1]
    depth = shared_gate.shape[0]
    if depth % LANES:
        slot = lax.axis_index("ep") * depth % LANES
        wide = jnp.zeros((LANES, shared_gate.shape[1]), BF16)
        shared_gate = lax.dynamic_update_slice_in_dim(wide, shared_gate, slot, 0)
        shared_up = lax.dynamic_update_slice_in_dim(wide, shared_up, slot, 0)
    return layer(
        ranks_ep,
        ranks_tp,
        tokens,
        lengths,
        cache,
        attn_gain.reshape(1, width),
        query_weight,
        key_weight,
        value_weight,
        stick_bias,
        out_weight,
        ffn_gain.reshape(1, width),
        routes.T,
        route_weights.T,
        expert_gate,
        expert_up,
        expert_down,
        shared_gate,
        shared_up,
        shared_down,
        gate_vector,
    )


def solution(mesh):
    placed = (
        P("ep", None),
        P("ep"),
        P("ep", None, "tp"),
        P(),
        P(None, "tp"),
        P(None, "tp"),
        P(None, "tp"),
        P("tp"),
        P("tp", None),
        P(),
        P("ep", None),
        P("ep", None),
        P("ep", None, "tp"),
        P("ep", None, "tp"),
        P("ep", "tp", None),
        P("ep", "tp"),
        P("ep", "tp"),
        P("tp", None),
        P(),
    )
    return jax.shard_map(
        functools.partial(shards, mesh.shape["ep"], mesh.shape["tp"]),
        mesh=mesh,
        in_specs=placed,
        out_specs=(P("ep", "tp"), P("ep", "tp")),
        check_vma=False,
    )
```

time: 60.4 us -> 43.1 us (0.71)
  Pallas kernels: 51 us -> 39.6 us
  matrix products: 4.89 us -> 0 us
  other arithmetic: 2.63 us -> 0 us
  local copies, waits for them, and re-layouts: 0.89 us -> 2.67 us
    pallas_call x2 -> x1, Pallas kernels: 51 us -> 39.6 us  [layer(): pl.pallas_call(functools.partial(layer_kernel, ranks_ep, ranks_tp), out_s...]
    dot_general x4 -> x0, matrix products: 4.89 us -> none  [the longest x1 2.69 us: shards(): jnp.dot(normed, query_weight, preferred_element_type=F32).astype(BF16)]
    unnamed x10 -> x2, local copies, waits for them, and re-layouts: 0.02 us -> 2.67 us
    convert_element_type x1 -> x0, other arithmetic: 1.46 us -> none  [shards(): return (layer_out.astype(BF16), new_kv)]
    reduce_sum x1 -> x0, other arithmetic: 1.12 us -> none  [rms_scale(): jnp.mean(values_f * values_f, axis=-1, keepdims=True) + epsilon]
    reshape x1 -> x0, local copies, waits for them, and re-layouts: 0.69 us -> none  [shards(): new_kv = jnp.stack([key_rows.reshape(row_count, heads, HEAD_DIM), value_r...]
where the time goes in v1:
time: 43.1 us; the launch traced here: 42.9 us
  Pallas kernels  39.6 us (92%)
  local copies, waits for them, and re-layouts  2.67 us (6%)
  between operations  0.65 us (2%)
    pallas_call x1, Pallas kernels, layer(): pl.pallas_call(functools.partial(layer_kernel, ranks_ep, ranks_tp), out_s...  39.6 us
    unnamed x2, local copies, waits for them, and re-layouts  2.67 us

profile of v1, /device:TPU:0, one launch (start us, length us, event | category | flops | bytes accessed | tf_op | source)
XLA Modules:
  0.0 42.9 jit_solution(6594921774141264350)
XLA Ops:
  0.6 39.6 %shard_map.194 = (bf16[16,1024]{1,0:T(8,128)(2,1)}, bf16[16,256]{1,0:T(8,128)(2,1)}) custom-call(bf16[16,2048]{1,0:T(8,128)(2,1)} %tokens_hbm.1, s32[16]{0:T(128)} %lengths_hbm.1, bf16[16,1024,256]{2,1,0:T(8,128)(2,1)} %cache_hbm.1, f32[1,2048]{1,0:T(1,128)} %bitcast.4, bf16[2048,512]{1,0:T(8,128)(2,1)} %query_hbm.1, bf16[2048,128]{1,0:T(8,128)(2,1)} %key_hbm.1, ...), custom_call_target="tpu_custom_call" | custom-call | tf_op jit(solution)/shard_map/pallas_call | solution.py:606
  40.2 1.4 %copy.23 = bf16[16,1024]{1,0:T(8,128)(2,1)} copy(bf16[16,1024]{1,0:T(8,128)(2,1)} %get-tuple-element.4) | data formatting | bytes 65536
  41.6 1.3 %copy.24 = bf16[16,256]{1,0:T(8,128)(2,1)} copy(bf16[16,256]{1,0:T(8,128)(2,1)} %get-tuple-element.5) | data formatting | bytes 16384
